TPU v7x, 32 devices: a whole 2x2x4 slice. The times are simulated.
32 devices in a mesh: dp: 4 (over y, x), kv: 4 (over z), tp: 2 (over core).
Axes of the slice: x: 2, y: 2, z: 4, core: 2. Of those that a mesh axis runs over, the one named last changes fastest.
Arguments:
- tokens: bfloat16 [32, 4096], P('dp', ('kv', 'tp')), as said below
- query_weight: bfloat16 [4096, 16, 128], P(None, 'tp', 'kv'), may hold values from -0.09375 to 0.09375
- key_weight: bfloat16 [4096, 16, 128], P(None, 'tp', 'kv'), may hold values from -0.09375 to 0.09375
- value_weight: bfloat16 [4096, 16, 256], P(None, 'tp', 'kv'), may hold values from -0.09375 to 0.09375
- gate_weight: bfloat16 [4096, 16, 256], P(None, 'tp', 'kv'), may hold values from -0.09375 to 0.09375
- decay_weight: bfloat16 [4096, 16, 128], P(None, 'tp', 'kv'), may hold values from -0.09375 to 0.09375
- decay_bias: float32 [16, 128], P('tp'), may hold values from -8 to 2
- states: float32 [32, 16, 128, 256], P(('dp', 'kv'), 'tp'), may hold values from -4 to 4
- head_gain: float32 [16, 256], P('tp'), may hold values from 0.1 to 1.9
- out_weight: bfloat16 [4096, 4096], P(None, ('kv', 'tp')), as said below
- norm1_gain: float32 [4096], P(('kv', 'tp')), may hold values from 0.1 to 1.9
- norm1_bias: float32 [4096], P(('kv', 'tp')), may hold values from -3 to 3
- up_weight: bfloat16 [4096, 16384], P(None, ('kv', 'tp')), may hold values from -0.09375 to 0.09375
- down_weight: bfloat16 [16384, 4096], P(('kv', 'tp')), as said below
- norm2_gain: float32 [4096], P(('kv', 'tp')), may hold values from 0.1 to 1.9
- norm2_bias: float32 [4096], P(('kv', 'tp')), may hold values from -3 to 3
Outputs:
- layer_out: bfloat16 [32, 4096], P('dp', ('kv', 'tp'))
- new_states: float32 [32, 16, 128, 256], P(('dp', 'kv'), 'tp')
Inputs may be any that keep to these rules, and one draw needn't show every extreme that they name: `tokens`: each block of 64 features has its own scale. `out_weight`: entries lie within 13 / sqrt(4096) of zero. `down_weight`: entries lie within 14 / sqrt(16384) of zero.
All inputs are finite; a program needn't handle non-finite values.
Results may differ from a plain program's by a relative error of at most 0.009.
Values may be sent and summed in bfloat16 or wider, within the bound.
A program may use at most 128 MiB of HBM per device.

v0:
```python
import functools

import jax
import jax.numpy as jnp
from jax import lax
from jax.experimental import pallas as pl
from jax.experimental.pallas import tpu as pltpu
from jax.sharding import PartitionSpec as P

D = 4096
KEY_DIM = 128


ALPHA = 2.0**0.5
TAU = 16.0
LN_EPS = 1e-05
RMS_EPS = 1e-06


def project_flat(inputs, weight):
    flattened = weight.reshape(weight.shape[0], -1)
    return jnp.dot(inputs, flattened, preferred_element_type=jnp.float32).astype(jnp.bfloat16)


def normalize(inputs, average, spread, row_gain, row_shift):
    return ((inputs - average) * lax.rsqrt(spread + LN_EPS) * row_gain + row_shift).astype(
        jnp.bfloat16
    )


def body(
    tokens,
    query_weight,
    key_weight,
    value_weight,
    gate_weight,
    decay_weight,
    decay_bias,
    states,
    head_gain,
    out_weight,
    norm1_gain,
    norm1_bias,
    up_weight,
    down_weight,
    norm2_gain,
    norm2_bias,
):
    whole = lax.all_gather(tokens, ("kv", "tp"), axis=1, tiled=True)
    weights_list = (query_weight, key_weight, decay_weight, value_weight, gate_weight)
    packed = jnp.concatenate([project_flat(whole, weight) for weight in weights_list], axis=1)
    arrived = lax.all_to_all(packed, "kv", split_axis=0, concat_axis=0, tiled=True)
    groups = lax.axis_size("kv")
    seq_count = whole.shape[0] // groups
    local_heads = query_weight.shape[1]
    unpacked = []
    start = 0
    for weight in weights_list:
        channels = weight.shape[2]
        width = local_heads * channels
        block = arrived[:, start : start + width].reshape(groups, seq_count, local_heads, channels)
        block = block.transpose(1, 2, 0, 3).reshape(seq_count, local_heads, groups * channels)
        unpacked.append(block.astype(jnp.float32))
        start = start + width
    query_rows = unpacked[0] * KEY_DIM ** (-0.5)
    key_rows = unpacked[1]
    decay_rows = unpacked[2]
    value_rows = unpacked[3]
    gate_rows = unpacked[4]
    retain = jnp.exp(jax.nn.log_sigmoid(decay_rows + decay_bias) / TAU)
    new_states = retain[..., None] * states + key_rows[..., :, None] * value_rows[..., None, :]
    readout = jnp.einsum("shk,shkv->shv", query_rows, new_states, precision=lax.Precision.HIGHEST)
    readout = (
        readout
        * lax.rsqrt(jnp.mean(readout * readout, axis=-1, keepdims=True) + RMS_EPS)
        * head_gain
    )
    attended = (readout * jax.nn.silu(gate_rows)).astype(jnp.bfloat16)
    seq_count, local_heads, value_width = attended.shape
    flat_width = local_heads * value_width
    collected = lax.all_gather(
        attended.reshape(1, seq_count, flat_width), ("kv", "tp"), axis=0, tiled=True
    )
    halves = lax.axis_size("tp")
    collected = collected.reshape(-1, halves, seq_count, flat_width)
    columns = out_weight.shape[1]
    out_parts = out_weight.reshape(halves, flat_width, columns)
    mixed_heads = jnp.einsum(
        "atsc,tcd->asd", collected, out_parts, preferred_element_type=jnp.float32
    ).reshape(-1, columns)
    residual_one = ALPHA * tokens.astype(jnp.float32) + mixed_heads
    offset = lax.axis_index(("kv", "tp")) * columns
    totals = lax.psum(
        (
            jnp.sum(residual_one, axis=-1, keepdims=True),
            jnp.sum(residual_one * residual_one, axis=-1, keepdims=True),
        ),
        ("kv", "tp"),
    )
    average = totals[0] / D
    spread = totals[1] / D - average * average
    normed_own = normalize(residual_one, average, spread, norm1_gain, norm1_bias)
    normed = lax.all_gather(normed_own, ("kv", "tp"), axis=1, tiled=True)
    lifted = jnp.dot(normed, up_weight, preferred_element_type=jnp.float32)
    hidden = jnp.square(jax.nn.relu(lifted)).astype(jnp.bfloat16)
    mixer_term = jnp.dot(hidden, down_weight, preferred_element_type=jnp.float32)
    mixer_all = lax.psum(mixer_term, ("kv", "tp"))
    residual_two = ALPHA * normed.astype(jnp.float32) + mixer_all
    average = jnp.sum(residual_two, axis=-1, keepdims=True) / D
    spread = jnp.sum(residual_two * residual_two, axis=-1, keepdims=True) / D - average * average
    own_rows = lax.dynamic_slice_in_dim(residual_two, offset, columns, 1)
    layer_out = normalize(own_rows, average, spread, norm2_gain, norm2_bias)
    return (layer_out, new_states)


MESH = pl.DeviceIdType.MESH
F32 = jnp.float32
BF16 = jnp.bfloat16


def dot_nt(left, right):
    return lax.dot_general(left, right, (((1,), (1,)), ((), ())), preferred_element_type=F32)


def layer_kernel(
    groups, halves, tokens, wq, wk, wd, wv, wg, bias, states, head_gain, wout, gain1, shift1,
    wup, wdown, gain2, shift2,
    out, states_out,
    tok_v, proj_v, out_v, up_v, down_v, state_v, bias_v, hgain_v, gain1_v, shift1_v, gain2_v,
    shift2_v, own_g1, own_s1, bias_t, x_v, a_send, a_recv, a_rows, att_rows, gate_rows, att_send, att_recv,
    x_rows, r_own, r_all, normed_v, hidden_v, p_send, p_recv, s_send, s_recv, res_v,
    load_sem, x_ss, x_rs, a_ss, a_rs, t_ss, t_rs, r_ss, r_rs, p_ss, p_rs, s_ss, s_rs, g_ss, g_rs,
    b_ss, b_rs, c_ss, c_rs,
):
    members = groups * halves
    my_kv, my_tp = lax.axis_index("kv"), lax.axis_index("tp")
    me = my_kv * halves + my_tp
    rows, cols = tok_v.shape
    width = x_v.shape[1]
    seqs = rows // groups
    heads, kdim = bias_v.shape
    vdim = hgain_v.shape[1]
    kc, vc = kdim // groups, vdim // groups
    nk, nv = heads * kc, heads * vc

    def load(index, src, dst):
        copy = pltpu.make_async_copy(src, dst, load_sem.at[index])
        copy.start()
        return copy

    loads = {}
    loads["tok"] = load(0, tokens, tok_v)
    loads["g1"] = load(1, gain1, own_g1)
    loads["s1"] = load(2, shift1, own_s1)
    loads["bias"] = load(3, bias, bias_v)
    start = 0
    for index, (name, weight) in enumerate((("q", wq), ("k", wk), ("d", wd), ("v", wv), ("g", wg))):
        size = weight.shape[0]
        loads[name] = load(4 + index, weight, proj_v.at[pl.ds(start, size)])
        start += size
    loads["hg"] = load(9, head_gain, hgain_v)
    loads["g2"] = load(10, gain2, gain2_v)
    loads["s2"] = load(11, shift2, shift2_v)
    loads["st"] = load(12, states, state_v)
    loads["out"] = load(13, wout, out_v)
    loads["up"] = load(14, wup, up_v)
    loads["down"] = load(15, wdown, down_v)

    def member(offset):
        index = lax.rem(me + offset, members)
        return index, {"kv": index // halves, "tp": lax.rem(index, halves)}

    def block(index):
        return pl.ds(pl.multiple_of(index * cols, cols), cols)

    barrier = pltpu.get_barrier_semaphore()
    for o in range(1, members):
        pl.semaphore_signal(barrier, inc=1, device_id=member(o)[1], device_id_type=MESH)
    pl.semaphore_wait(barrier, members - 1)

    def remote(src, dst, send, recv, target):
        return pltpu.make_async_remote_copy(
            src_ref=src, dst_ref=dst, send_sem=send, recv_sem=recv, device_id=target,
            device_id_type=MESH,
        )

    def spread(src, place, send, recv):
        copies = []
        for o in range(1, members):
            copy = remote(src, place(me), send.at[o], recv.at[o], member(o)[1])
            copy.start()
            copies.append(copy)
        return copies

    def collect(src, place, send, recv):
        for o in range(1, members):
            source, target = member(members - o)
            remote(src, place(source), send.at[o], recv.at[o], target).wait_recv()

    pending = []
    loads["tok"].wait()
    pending += spread(tok_v, lambda i: x_v.at[:, block(i)], x_ss, x_rs)
    x_v[:, block(me)] = tok_v[...]

    loads["bias"].wait()
    turned = jnp.concatenate([bias_v[...], jnp.zeros((kdim - heads, kdim), F32)], axis=0).T
    lane = lax.broadcasted_iota(jnp.int32, (kc, rows), 1)
    for h in range(heads):
        piece = jnp.zeros((kc, rows), F32)
        for b in range(groups):
            here = (lane >= b * seqs) & (lane < (b + 1) * seqs)
            piece = jnp.where(here, turned[b * kc : (b + 1) * kc, h : h + 1], piece)
        bias_t[h * kc : (h + 1) * kc, :] = piece

    collect(tok_v, lambda i: x_v.at[:, block(i)], x_ss, x_rs)
    loads["g1"].wait()
    loads["s1"].wait()
    pending += spread(own_g1, lambda i: gain1_v.at[:, block(i)], g_ss, g_rs)
    pending += spread(own_s1, lambda i: shift1_v.at[:, block(i)], b_ss, b_rs)
    gain1_v[:, block(me)] = own_g1[...]
    shift1_v[:, block(me)] = own_s1[...]
    x_all = x_v[...]

    def store_projection(first, size):
        got = dot_nt(x_all, proj_v[first : first + size, :]).astype(BF16).astype(F32)
        for a in range(groups):
            a_send[a, :, first : first + size] = got[a * seqs : (a + 1) * seqs, :]

    def exchange(part, send, recv):
        for o in range(1, groups):
            peer = lax.rem(my_kv + o, groups)
            copy = remote(
                a_send.at[peer, :, part], a_recv.at[my_kv, :, part], send.at[o], recv.at[o],
                {"kv": peer, "tp": my_tp},
            )
            copy.start()
            pending.append(copy)

    def arrive(part, send, recv):
        for o in range(1, groups):
            peer = lax.rem(my_kv + groups - o, groups)
            remote(
                a_send.at[peer, :, part], a_recv.at[peer, :, part], send.at[o], recv.at[o],
                {"kv": peer, "tp": my_tp},
            ).wait_recv()
        for b in range(groups):
            a_rows[b * seqs : (b + 1) * seqs, part] = a_recv[b, :, part]

    early, late = slice(0, 3 * nk + nv), slice(3 * nk + nv, 3 * nk + 2 * nv)
    loads["q"].wait()
    loads["k"].wait()
    store_projection(0, 2 * nk)
    loads["d"].wait()
    loads["v"].wait()
    store_projection(2 * nk, nk + nv)
    exchange(early, a_ss, a_rs)
    loads["g"].wait()
    store_projection(3 * nk + nv, nv)
    exchange(late, c_ss, c_rs)
    a_recv[my_kv] = a_send[my_kv]
    arrive(early, a_ss, a_rs)
    qt = a_rows[:, 0:nk].T * KEY_DIM ** (-0.5)
    kt = a_rows[:, nk : 2 * nk].T
    zt = a_rows[:, 2 * nk : 3 * nk].T + bias_t[...]
    rt = jnp.exp((jnp.minimum(zt, 0.0) - jnp.log1p(jnp.exp(-jnp.abs(zt)))) / TAU)
    loads["st"].wait()
    for s in range(seqs):
        for h in range(heads):
            first = 3 * nk + h * vc
            values = []
            for b in range(groups):
                row = b * seqs + s
                values.append(a_rows[row : row + 1, first : first + vc])
            value = jnp.concatenate(values, axis=1)
            total = None
            for b in range(groups):
                lanes = slice(b * seqs + s, b * seqs + s + 1)
                subs = slice(h * kc, (h + 1) * kc)
                fresh = (
                    rt[subs, lanes] * state_v[s, h, b * kc : (b + 1) * kc, :]
                    + kt[subs, lanes] * value
                )
                state_v[s, h, b * kc : (b + 1) * kc, :] = fresh
                term = qt[subs, lanes] * fresh
                total = term if total is None else total + term
            att_rows[s : s + 1, h * vdim : (h + 1) * vdim] = jnp.sum(total, axis=0, keepdims=True)
    loads["hg"].wait()
    arrive(late, c_ss, c_rs)
    for s in range(seqs):
        for h in range(heads):
            first = 3 * nk + nv + h * vc
            gates = [
                a_rows[b * seqs + s : b * seqs + s + 1, first : first + vc] for b in range(groups)
            ]
            gate_rows[s : s + 1, h * vdim : (h + 1) * vdim] = jnp.concatenate(gates, axis=1)
    for h in range(heads):
        span = slice(h * vdim, (h + 1) * vdim)
        readout = att_rows[:, span]
        gate = gate_rows[:, span]
        power = jnp.mean(readout * readout, axis=-1, keepdims=True)
        readout = readout * lax.rsqrt(power + RMS_EPS) * hgain_v[h : h + 1, :]
        att_send[:, span] = (readout * (gate / (1.0 + jnp.exp(-gate)))).astype(BF16)

    pending += spread(att_send, lambda i: att_recv.at[i], t_ss, t_rs)
    save = pltpu.make_async_copy(state_v, states_out, load_sem.at[16])
    save.start()
    att_recv[me] = att_send[...]
    collect(att_send, lambda i: att_recv.at[i], t_ss, t_rs)
    half = heads * vdim
    for a in range(groups):
        for t in range(halves):
            x_rows[a * seqs : (a + 1) * seqs, t * half : (t + 1) * half] = att_recv[a * halves + t].astype(F32)
    loads["out"].wait()
    mixed = jnp.dot(x_rows[...].astype(BF16), out_v[...], preferred_element_type=F32)
    r_own[...] = ALPHA * tok_v[...].astype(F32) + mixed
    pending += spread(r_own, lambda i: r_all.at[:, block(i)], r_ss, r_rs)
    r_all[:, block(me)] = r_own[...]
    collect(own_g1, lambda i: gain1_v.at[:, block(i)], g_ss, g_rs)
    collect(own_s1, lambda i: shift1_v.at[:, block(i)], b_ss, b_rs)
    collect(r_own, lambda i: r_all.at[:, block(i)], r_ss, r_rs)
    whole = r_all[...]
    average = jnp.sum(whole, axis=-1, keepdims=True) / width
    spread_one = jnp.sum(whole * whole, axis=-1, keepdims=True) / width - average * average
    normed = normalize(whole, average, spread_one, gain1_v[...], shift1_v[...])
    normed_v[...] = normed

    loads["up"].wait()
    units = up_v.shape[1]
    step = min(units, 512)

    def lift(i, carry):
        span = pl.ds(pl.multiple_of(i * step, step), step)
        lifted = jnp.dot(normed_v[...], up_v[:, span], preferred_element_type=F32)
        hidden_v[:, span] = jnp.square(jnp.maximum(lifted, 0.0)).astype(BF16)
        return carry

    lax.fori_loop(0, units // step, lift, 0)
    loads["down"].wait()

    def drop(o, carry):
        index, target = member(o)
        p_send[o] = jnp.dot(hidden_v[...], down_v[:, block(index)], preferred_element_type=F32)
        remote(p_send.at[o], p_recv.at[o], p_ss.at[o], p_rs.at[o], target).start()
        return carry

    lax.fori_loop(1, members, drop, 0)
    total = jnp.dot(hidden_v[...], down_v[:, block(me)], preferred_element_type=F32)
    total = total + ALPHA * normed_v[:, block(me)].astype(F32)
    for o in range(1, members):
        target = member(members - o)[1]
        remote(p_send.at[o], p_recv.at[o], p_ss.at[o], p_rs.at[o], target).wait_recv()
        total = total + p_recv[o]
    sums = jnp.sum(total, axis=-1, keepdims=True)
    squares = jnp.sum(total * total, axis=-1, keepdims=True)
    lane = lax.broadcasted_iota(jnp.int32, s_send.shape, 1)
    stats = jnp.where(lane == 0, sums, squares)
    s_send[...] = stats
    pending += spread(s_send, lambda i: s_recv.at[i], s_ss, s_rs)
    loads["g2"].wait()
    loads["s2"].wait()
    for o in range(1, members):
        source, target = member(members - o)
        remote(s_send, s_recv.at[source], s_ss.at[o], s_rs.at[o], target).wait_recv()
        stats = stats + s_recv[source]
    average = stats[:, 0:1] / width
    spread_two = stats[:, 1:2] / width - average * average
    res_v[...] = normalize(total, average, spread_two, gain2_v[...], shift2_v[...])
    result = pltpu.make_async_copy(res_v, out, load_sem.at[17])
    result.start()
    for copy in pending:
        copy.wait_send()
    for o in range(1, members):
        remote(p_send.at[o], p_recv.at[o], p_ss.at[o], p_rs.at[o], member(o)[1]).wait_send()
    save.wait()
    result.wait()


def finish_kernel(result, fresh, out, states_out, res_v, state_v, sems):
    heads = fresh.shape[1]
    takes = [pltpu.make_async_copy(result, res_v, sems.at[0, heads])]
    puts = [pltpu.make_async_copy(res_v, out, sems.at[1, heads])]
    for h in range(heads):
        takes.append(pltpu.make_async_copy(fresh.at[:, h], state_v.at[:, h], sems.at[0, h]))
        puts.append(pltpu.make_async_copy(state_v.at[:, h], states_out.at[:, h], sems.at[1, h]))
    for take in takes:
        take.start()
    for take, put in zip(takes, puts):
        take.wait()
        put.start()
    for put in puts:
        put.wait()


def fused(groups, halves, *arrays):
    (tokens, wq, wk, wv, wg, wd, bias, states, head_gain, wout, gain1, shift1, wup, wdown, gain2,
     shift2) = arrays

    def flat(weight):
        return weight.transpose(1, 2, 0).reshape(-1, weight.shape[0])

    def row(vector):
        return vector.reshape(1, -1)

    rows, cols = tokens.shape
    members = groups * halves
    width = wq.shape[0]
    seqs, heads, kdim, vdim = states.shape
    proj = 3 * wq.shape[1] * wq.shape[2] + 2 * wv.shape[1] * wv.shape[2]
    vmem = pltpu.VMEM
    dma = pltpu.SemaphoreType.DMA
    anywhere = pl.BlockSpec(memory_space=pl.ANY)
    scratch = [
        vmem((rows, cols), BF16),
        vmem((proj, width), BF16),
        vmem(wout.shape, BF16),
        vmem(wup.shape, BF16),
        vmem(wdown.shape, BF16),
        vmem(states.shape, F32),
        vmem(bias.shape, F32),
        vmem(head_gain.shape, F32),
        vmem((1, width), F32),
        vmem((1, width), F32),
        vmem((1, cols), F32),
        vmem((1, cols), F32),
        vmem((1, cols), F32),
        vmem((1, cols), F32),
        vmem((heads * kdim // groups, rows), F32),
        vmem((rows, width), BF16),
        vmem((groups, seqs, proj), F32),
        vmem((groups, seqs, proj), F32),
        vmem((rows, proj), F32),
        vmem((seqs, heads * vdim), F32),
        vmem((seqs, heads * vdim), F32),
        vmem((seqs, heads * vdim), BF16),
        vmem((members, seqs, heads * vdim), BF16),
        vmem((rows, halves * heads * vdim), F32),
        vmem((rows, cols), F32),
        vmem((rows, width), F32),
        vmem((rows, width), BF16),
        vmem((rows, wup.shape[1]), BF16),
        vmem((members, rows, cols), F32),
        vmem((members, rows, cols), F32),
        vmem((rows, 128), F32),
        vmem((members, rows, 128), F32),
        vmem((rows, cols), BF16),
        dma((18,)),
    ]
    for count in (members, groups, *[members] * 6, groups):
        scratch += [dma((count,)), dma((count,))]
    result, fresh = pl.pallas_call(
        functools.partial(layer_kernel, groups, halves),
        out_shape=(
            jax.ShapeDtypeStruct(tokens.shape, BF16),
            jax.ShapeDtypeStruct(states.shape, F32),
        ),
        in_specs=[anywhere] * 16,
        out_specs=(anywhere, anywhere),
        scratch_shapes=scratch,
        compiler_params=pltpu.CompilerParams(
            collective_id=0, has_side_effects=True, vmem_limit_bytes=67043328
        ),
    )(
        tokens, flat(wq), flat(wk), flat(wd), flat(wv), flat(wg), bias, states, head_gain, wout,
        row(gain1), row(shift1), wup, wdown, row(gain2), row(shift2),
    )
    return pl.pallas_call(
        finish_kernel,
        out_shape=(
            jax.ShapeDtypeStruct(tokens.shape, BF16),
            jax.ShapeDtypeStruct(states.shape, F32),
        ),
        in_specs=[anywhere] * 2,
        out_specs=(anywhere, anywhere),
        scratch_shapes=[vmem(tokens.shape, BF16), vmem(states.shape, F32), dma((2, heads + 1))],
        compiler_params=pltpu.CompilerParams(vmem_limit_bytes=67043328),
    )(result, fresh)


def dispatch(groups, halves, *arrays):
    rows, cols = arrays[0].shape
    if rows == 8 and cols % 128 == 0 and rows % groups == 0:
        return fused(groups, halves, *arrays)
    return body(*arrays)


def solution(mesh):
    placed = (
        P("dp", ("kv", "tp")),
        P(None, "tp", "kv"),
        P(None, "tp", "kv"),
        P(None, "tp", "kv"),
        P(None, "tp", "kv"),
        P(None, "tp", "kv"),
        P("tp", None),
        P(("dp", "kv"), "tp", None, None),
        P("tp", None),
        P(None, ("kv", "tp")),
        P(("kv", "tp")),
        P(("kv", "tp")),
        P(None, ("kv", "tp")),
        P(("kv", "tp"), None),
        P(("kv", "tp")),
        P(("kv", "tp")),
    )
    return jax.shard_map(
        functools.partial(dispatch, mesh.shape["kv"], mesh.shape["tp"]),
        mesh=mesh,
        in_specs=placed,
        out_specs=(P("dp", ("kv", "tp")), P(("dp", "kv"), "tp", None, None)),
        check_vma=False,
    )
```

profile of v0, /device:TPU:0, one launch (start us, length us, event | category | flops | bytes accessed | tf_op | source)
XLA Modules:
  0.0 44.0 jit_solution(8337567144860576662)
XLA Ops:
  0.6 40.9 %shard_map.167 = (bf16[8,512]{1,0:T(8,128)(2,1)}, f32[2,8,128,256]{3,2,1,0:T(8,128)}) custom-call(bf16[8,512]{1,0:T(8,128)(2,1)} %tokens.1, bf16[256,4096]{1,0:T(8,128)(2,1)} %bitcast.21, bf16[256,4096]{1,0:T(8,128)(2,1)} %bitcast.22, bf16[256,4096]{1,0:T(8,128)(2,1)} %bitcast.23, bf16[512,4096]{1,0:T(8,128)(2,1)} %bitcast.19, bf16[512,4096]{1,0:T(8,128)(2,1)} %bitcast.20, ...), custom_call_target="tpu_custom_call" | custom-call | tf_op jit(solution)/shard_map/pallas_call | solution.py:450
  41.6 2.4 %shard_map.168 = (bf16[8,512]{1,0:T(8,128)(2,1)}, f32[2,8,128,256]{3,2,1,0:T(8,128)}) custom-call(bf16[8,512]{1,0:T(8,128)(2,1)} %get-tuple-element.4.result, f32[2,8,128,256]{3,2,1,0:T(8,128)} %get-tuple-element.5.fresh), custom_call_target="tpu_custom_call" | custom-call | tf_op jit(solution)/shard_map/pallas_call | solution.py:466
where the time goes:
time: 44.2 us; the launch traced here: 44 us
  Pallas kernels  43.4 us (98%)
  between operations  0.64 us (1%)
    pallas_call x1, Pallas kernels, fused(): pl.pallas_call(functools.partial(layer_kernel, groups, halves), out_shape...  40.9 us
    pallas_call x1, Pallas kernels, fused(): pl.pallas_call(finish_kernel, out_shape=(jax.ShapeDtypeStruct(tokens.shap...  2.43 us

commit v1 on v0

v1 whole, which is shorter than its diff:
```python
import functools

import jax
import jax.numpy as jnp
from jax import lax
from jax.experimental import pallas as pl
from jax.experimental.pallas import tpu as pltpu
from jax.sharding import PartitionSpec as P

D = 4096
KEY_DIM = 128


ALPHA = 2.0**0.5
TAU = 16.0
LN_EPS = 1e-05
RMS_EPS = 1e-06


def project_flat(inputs, weight):
    flattened = weight.reshape(weight.shape[0], -1)
    return jnp.dot(inputs, flattened, preferred_element_type=jnp.float32).astype(jnp.bfloat16)


def normalize(inputs, average, spread, row_gain, row_shift):
    return ((inputs - average) * lax.rsqrt(spread + LN_EPS) * row_gain + row_shift).astype(
        jnp.bfloat16
    )


def body(
    tokens,
    query_weight,
    key_weight,
    value_weight,
    gate_weight,
    decay_weight,
    decay_bias,
    states,
    head_gain,
    out_weight,
    norm1_gain,
    norm1_bias,
    up_weight,
    down_weight,
    norm2_gain,
    norm2_bias,
):
    whole = lax.all_gather(tokens, ("kv", "tp"), axis=1, tiled=True)
    weights_list = (query_weight, key_weight, decay_weight, value_weight, gate_weight)
    packed = jnp.concatenate([project_flat(whole, weight) for weight in weights_list], axis=1)
    arrived = lax.all_to_all(packed, "kv", split_axis=0, concat_axis=0, tiled=True)
    groups = lax.axis_size("kv")
    seq_count = whole.shape[0] // groups
    local_heads = query_weight.shape[1]
    unpacked = []
    start = 0
    for weight in weights_list:
        channels = weight.shape[2]
        width = local_heads * channels
        block = arrived[:, start : start + width].reshape(groups, seq_count, local_heads, channels)
        block = block.transpose(1, 2, 0, 3).reshape(seq_count, local_heads, groups * channels)
        unpacked.append(block.astype(jnp.float32))
        start = start + width
    query_rows = unpacked[0] * KEY_DIM ** (-0.5)
    key_rows = unpacked[1]
    decay_rows = unpacked[2]
    value_rows = unpacked[3]
    gate_rows = unpacked[4]
    retain = jnp.exp(jax.nn.log_sigmoid(decay_rows + decay_bias) / TAU)
    new_states = retain[..., None] * states + key_rows[..., :, None] * value_rows[..., None, :]
    readout = jnp.einsum("shk,shkv->shv", query_rows, new_states, precision=lax.Precision.HIGHEST)
    readout = (
        readout
        * lax.rsqrt(jnp.mean(readout * readout, axis=-1, keepdims=True) + RMS_EPS)
        * head_gain
    )
    attended = (readout * jax.nn.silu(gate_rows)).astype(jnp.bfloat16)
    seq_count, local_heads, value_width = attended.shape
    flat_width = local_heads * value_width
    collected = lax.all_gather(
        attended.reshape(1, seq_count, flat_width), ("kv", "tp"), axis=0, tiled=True
    )
    halves = lax.axis_size("tp")
    collected = collected.reshape(-1, halves, seq_count, flat_width)
    columns = out_weight.shape[1]
    out_parts = out_weight.reshape(halves, flat_width, columns)
    mixed_heads = jnp.einsum(
        "atsc,tcd->asd", collected, out_parts, preferred_element_type=jnp.float32
    ).reshape(-1, columns)
    residual_one = ALPHA * tokens.astype(jnp.float32) + mixed_heads
    offset = lax.axis_index(("kv", "tp")) * columns
    totals = lax.psum(
        (
            jnp.sum(residual_one, axis=-1, keepdims=True),
            jnp.sum(residual_one * residual_one, axis=-1, keepdims=True),
        ),
        ("kv", "tp"),
    )
    average = totals[0] / D
    spread = totals[1] / D - average * average
    normed_own = normalize(residual_one, average, spread, norm1_gain, norm1_bias)
    normed = lax.all_gather(normed_own, ("kv", "tp"), axis=1, tiled=True)
    lifted = jnp.dot(normed, up_weight, preferred_element_type=jnp.float32)
    hidden = jnp.square(jax.nn.relu(lifted)).astype(jnp.bfloat16)
    mixer_term = jnp.dot(hidden, down_weight, preferred_element_type=jnp.float32)
    mixer_all = lax.psum(mixer_term, ("kv", "tp"))
    residual_two = ALPHA * normed.astype(jnp.float32) + mixer_all
    average = jnp.sum(residual_two, axis=-1, keepdims=True) / D
    spread = jnp.sum(residual_two * residual_two, axis=-1, keepdims=True) / D - average * average
    own_rows = lax.dynamic_slice_in_dim(residual_two, offset, columns, 1)
    layer_out = normalize(own_rows, average, spread, norm2_gain, norm2_bias)
    return (layer_out, new_states)


MESH = pl.DeviceIdType.MESH
F32 = jnp.float32
BF16 = jnp.bfloat16


def dot_nt(left, right):
    return lax.dot_general(left, right, (((1,), (1,)), ((), ())), preferred_element_type=F32)


def nearest(place, count, step):
    below, above = place, count - 1 - place
    pairs = jnp.minimum(below, above)
    away = (step + 1) // 2 * (1 if step % 2 else -1)
    zigzag = jnp.where(below <= above, place - away, place + away)
    onward = jnp.where(below < above, place + (step - pairs), place - (step - pairs))
    return jnp.where(step <= 2 * pairs, zigzag, onward)


def layer_kernel(
    groups, halves, tokens, wq, wk, wd, wv, wg, bias, states, head_gain, wout, gain1, shift1,
    wup, wdown, gain2, shift2,
    out, states_out,
    proj_v, out_v, up_v, down_v, state_v, bias_v, hgain_v, gain1_v, shift1_v, gain2_v, shift2_v,
    bias_rows, x_v, acc_v, a_send, a_recv, a_rows, att_send, att_recv, x_rows, mixed_v, const_v, u_v, moments_v, both_v,
    p_send, p_recv, finals_v,
    load_sem, proj_sem, up_sem, down_sem, ready, own_ss, x_rs, a_ss, a_rs, c_ss, c_rs, t_ss, t_rs,
    u_ss, u_rs, m_ss, m_rs, p_ss, p_rs, f_ss, f_rs,
):
    my_kv, my_tp = lax.axis_index("kv"), lax.axis_index("tp")
    me = my_kv * halves + my_tp
    members, rows, cols = x_v.shape
    width = members * cols
    span = halves * cols
    seqs = rows // groups
    heads, kdim = bias_v.shape
    vdim = hgain_v.shape[1]
    kc, vc = kdim // groups, vdim // groups
    nk, nv = heads * kc, heads * vc
    top = groups - 1
    chips = [nearest(my_kv, groups, step) for step in range(groups)]
    cores = [lax.rem(my_tp + o, halves) for o in range(halves)]

    def load(src, dst, sem):
        copy = pltpu.make_async_copy(src, dst, sem)
        copy.start()
        return copy

    def chunk(chip):
        return pl.ds(pl.multiple_of(chip * span, span), span)

    loads = {}
    for index, (name, src, dst) in enumerate((
        ("tok", tokens, x_v.at[me]), ("g1", gain1, gain1_v), ("s1", shift1, shift1_v), ("bias", bias, bias_v),
    )):
        loads[name] = load(src, dst, load_sem.at[index])

    proj_loads = []

    def load_projections(step, chip):
        start = 0
        for index, weight in enumerate((wq, wk, wd, wv, wg)):
            size = weight.shape[0]
            proj_loads.append(load(
                weight.at[:, chunk(chip)], proj_v.at[pl.ds(start, size), chunk(chip)], proj_sem.at[step, index]
            ))
            start += size

    load_projections(0, chips[0])
    barrier = pltpu.get_barrier_semaphore()

    def greet(kv, tp):
        pl.semaphore_signal(barrier, inc=1, device_id={"kv": kv, "tp": tp}, device_id_type=MESH)

    @pl.when(my_kv > 0)
    def _():
        for core in cores:
            greet(my_kv - 1, core)

    for core in cores[1:]:
        greet(my_kv, core)
    for d in range(1, groups):

        @pl.when(my_kv + d < groups)
        def _():
            for core in cores:
                greet(my_kv + d, core)

    def remote(src, dst, send, recv, kv, tp):
        return pltpu.make_async_remote_copy(
            src_ref=src, dst_ref=dst, send_sem=send, recv_sem=recv, device_id={"kv": kv, "tp": tp},
            device_id_type=MESH,
        )

    def own_copy(kv, core, slot):
        return remote(x_v.at[me], x_v.at[me], own_ss.at[slot], x_rs.at[me], kv, core)

    def own_sends(first):
        plans = []
        if first:
            for o, core in enumerate(cores):
                plans.append((my_kv < top, my_kv + 1, core, o))
            for d in range(top, 0, -1):
                for o, core in enumerate(cores):
                    plans.append((my_kv >= d, my_kv - d, core, (d + 1) * halves + o))
            for o, core in enumerate(cores[1:]):
                plans.append((None, my_kv, core, halves + o))
        else:
            for d in range(2, groups):
                for o, core in enumerate(cores):
                    plans.append((my_kv + d < groups, my_kv + d, core, (groups + d - 1) * halves + o))
        return plans

    def each_own(first, act):
        for condition, kv, core, slot in own_sends(first):
            if condition is None:
                act(own_copy(kv, core, slot))
            else:

                @pl.when(condition)
                def _():
                    act(own_copy(kv, core, slot))

    def send_far():
        for d in range(2, groups):

            @pl.when(my_kv + d < groups)
            def _():
                pl.semaphore_wait(ready.at[d], halves)
                for o, core in enumerate(cores):
                    own_copy(my_kv + d, core, (groups + d - 1) * halves + o).start()

    expected = (halves - 1) + halves * my_kv + jnp.where(my_kv < top, halves, 0)
    pl.semaphore_wait(barrier, expected)
    for d in range(2, groups):

        @pl.when(my_kv >= d)
        def _():
            for core in cores:
                pl.semaphore_signal(
                    ready.at[d], inc=1, device_id={"kv": my_kv - d, "tp": core}, device_id_type=MESH
                )

    loads["tok"].wait()
    each_own(True, lambda copy: copy.start())
    load_projections(1, chips[1])
    pending = []

    def everyone():
        targets = [(chip, core) for chip in reversed(chips[1:]) for core in cores]
        return targets + [(my_kv, core) for core in cores[1:]]

    def spread(buffer, send, recv):
        for o, (chip, core) in enumerate(everyone()):
            copy = remote(buffer.at[me], buffer.at[me], send.at[o], recv.at[me], chip, core)
            copy.start()
            pending.append(copy)

    def collect(buffer, recv, chip, core):
        block = chip * halves + core
        remote(buffer.at[block], buffer.at[block], recv.at[block], recv.at[block], my_kv, my_tp).wait_recv()

    late = []
    for step, chip in enumerate(chips):
        for core in cores if step else cores[1:]:
            collect(x_v, x_rs, chip, core)
        for index in range(5):
            proj_loads[step * 5 + index].wait()
        if step + 2 < groups:
            load_projections(step + 2, chips[step + 2])
        if step == max(groups - 2, 0):
            for index, (name, src, dst) in enumerate((
                ("hg", head_gain, hgain_v), ("g2", gain2, gain2_v), ("s2", shift2, shift2_v),
                ("st", states, state_v), ("out", wout, out_v),
            )):
                loads[name] = load(src, dst, load_sem.at[4 + index])
        if step == groups - 1:
            for index, to in enumerate(chips):
                late.append(load(wup.at[chunk(to), :], up_v.at[chunk(to), :], up_sem.at[index]))
        blocks = x_v[pl.ds(chip * halves, halves)]
        left = jnp.concatenate([blocks[o] for o in range(halves)], axis=1)
        term = dot_nt(left, proj_v[:, chunk(chip)])
        acc_v[...] = acc_v[...] + term if step else term
        if step == 0:
            send_far()
            loads["g1"].wait()
            loads["s1"].wait()
            loads["bias"].wait()
            whole_shift = shift1_v[...]
            coarse = whole_shift.astype(BF16).astype(F32)
            place = lax.broadcasted_iota(jnp.int32, (rows, cols), 0)
            consts = jnp.where(place == my_tp, gain1_v[...], 0.0)
            consts = jnp.where(place == halves, coarse, consts)
            consts = jnp.where(place == halves + 1, whole_shift - coarse, consts)
            const_v[me] = consts.astype(BF16)
            for h in range(heads):
                for b in range(groups):
                    piece = jnp.broadcast_to(bias_v[h : h + 1, b * kc : (b + 1) * kc], (seqs, kc))
                    bias_rows[b * seqs : (b + 1) * seqs, h * kc : (h + 1) * kc] = piece
        if step == groups - 2:
            spread(const_v, c_ss, c_rs)
    quarter = down_v.shape[0] // 4
    down_loads = [
        load(wdown.at[pl.ds(i * quarter, quarter)], down_v.at[pl.ds(i * quarter, quarter)], down_sem.at[i])
        for i in range(4)
    ]

    for a in range(groups):
        a_send[a] = acc_v[a * seqs : (a + 1) * seqs, :].astype(BF16)
    for o, peer in enumerate(reversed(chips[1:])):
        copy = remote(a_send.at[peer], a_recv.at[my_kv], a_ss.at[o], a_rs.at[my_kv], peer, my_tp)
        copy.start()
        pending.append(copy)
    a_recv[my_kv] = a_send[my_kv]
    loads["st"].wait()
    loads["hg"].wait()
    for peer in chips[1:]:
        remote(a_send.at[peer], a_recv.at[peer], a_ss.at[0], a_rs.at[peer], my_kv, my_tp).wait_recv()
    for b in range(groups):
        a_rows[b * seqs : (b + 1) * seqs, :] = a_recv[b].astype(F32)

    q = a_rows[:, 0:nk] * KEY_DIM ** (-0.5)
    k = a_rows[:, nk : 2 * nk]
    z = a_rows[:, 2 * nk : 3 * nk] + bias_rows[...]
    retain = jnp.exp((jnp.minimum(z, 0.0) - jnp.log1p(jnp.exp(-jnp.abs(z)))) / TAU)
    product = q * k
    met = product
    for b in range(1, groups):
        met = met + pltpu.roll(product, b * seqs, 0)
    turned = jnp.concatenate([q * retain, met], axis=1).T

    def wide(s, h, first):
        start = first + h * vc
        parts = [a_rows[b * seqs + s : b * seqs + s + 1, start : start + vc] for b in range(groups)]
        return jnp.concatenate(parts, axis=1)

    strength = jnp.concatenate(
        [jnp.sum(turned[nk + h * kc : nk + (h + 1) * kc, :], axis=0, keepdims=True) for h in range(heads)], axis=0
    )
    values = []
    for s in range(seqs):
        value = jnp.concatenate([wide(s, h, 3 * nk) for h in range(heads)], axis=0)
        gate = jnp.concatenate([wide(s, h, 3 * nk + nv) for h in range(heads)], axis=0)
        values.append(value)
        lines = []
        for h in range(heads):
            total = None
            for b in range(groups):
                lane = b * seqs + s
                term = turned[h * kc : (h + 1) * kc, lane : lane + 1] * state_v[s, h, b * kc : (b + 1) * kc, :]
                total = term if total is None else total + term
            lines.append(jnp.sum(total, axis=0, keepdims=True))
        readout = jnp.concatenate(lines, axis=0) + strength[:, s : s + 1] * value
        power = jnp.mean(readout * readout, axis=-1, keepdims=True)
        readout = readout * lax.rsqrt(power + RMS_EPS) * hgain_v[...]
        attended = readout * (gate / (1.0 + jnp.exp(-gate)))
        for h in range(heads):
            att_send[s : s + 1, h * vdim : (h + 1) * vdim] = attended[h : h + 1, :].astype(BF16)
    for o, (chip, core) in enumerate(everyone()):
        copy = remote(att_send, att_recv.at[me], t_ss.at[o], t_rs.at[me], chip, core)
        copy.start()
        pending.append(copy)
    att_recv[me] = att_send[...]

    later = jnp.concatenate([retain, k], axis=1).T
    for s in range(seqs):
        for h in range(heads):
            for b in range(groups):
                lane = b * seqs + s
                subs = slice(h * kc, (h + 1) * kc)
                keys = slice(nk + h * kc, nk + (h + 1) * kc)
                states_out[s, h, b * kc : (b + 1) * kc, :] = (
                    later[subs, lane : lane + 1] * state_v[s, h, b * kc : (b + 1) * kc, :]
                    + later[keys, lane : lane + 1] * values[s][h : h + 1, :]
                )

    half = heads * vdim

    loads["out"].wait()
    for step, chip in enumerate(chips):
        for core in cores if step else cores[1:]:
            collect(att_recv, t_rs, chip, core)
        for t in range(halves):
            x_rows[step * seqs : (step + 1) * seqs, t * half : (t + 1) * half] = att_recv[chip * halves + t].astype(F32)
    mixed = jnp.dot(x_rows[...].astype(BF16), out_v[...], preferred_element_type=F32)
    for step, chip in enumerate(chips):
        mixed_v[chip] = mixed[step * seqs : (step + 1) * seqs]
    mixed = jnp.concatenate([mixed_v[a] for a in range(groups)], axis=0)
    residual = ALPHA * x_v[me].astype(F32) + mixed

    lane = lax.broadcasted_iota(jnp.int32, (rows, 128), 1)
    line = lax.broadcasted_iota(jnp.int32, (rows, 128), 0)

    def moments(block):
        center = jnp.sum(block, axis=-1, keepdims=True) / cols
        moved = block - center
        return center, moved, jnp.sum(moved * moved, axis=-1, keepdims=True)

    def as_row(center, power):
        both = jnp.where(lane == line, center, 0.0) + jnp.where(lane == line + rows, power, 0.0)
        return jnp.sum(both, axis=0, keepdims=True)

    def as_columns(row):
        center = jnp.sum(jnp.where(lane == line, row, 0.0), axis=-1, keepdims=True)
        power = jnp.sum(jnp.where(lane == line + rows, row, 0.0), axis=-1, keepdims=True)
        return center, power

    def combine(pairs):
        average = sum(center for center, _ in pairs) / members
        powers = sum(power + cols * jnp.square(center - average) for center, power in pairs)
        return average, lax.rsqrt(powers / width + LN_EPS)

    center, moved, power = moments(residual)
    u_v[me] = (moved * gain1_v[...]).astype(BF16)
    moments_v[me] = as_row(center, power)
    spread(u_v, u_ss, u_rs)
    spread(moments_v, m_ss, m_rs)

    for step, chip in enumerate(chips):
        for core in cores if step else cores[1:]:
            collect(const_v, c_rs, chip, core)
    lifted = fixed = None
    pairs = []
    for step, chip in enumerate(chips):
        late[step].wait()
        for core in cores if step else cores[1:]:
            collect(u_v, u_rs, chip, core)
            collect(moments_v, m_rs, chip, core)
        left = []
        for o in range(halves):
            block = chip * halves + o
            left.append(jnp.concatenate([u_v[block], const_v[block]], axis=0))
            pairs.append(as_columns(moments_v[block]))
        term = jnp.dot(jnp.concatenate(left, axis=1), up_v[chunk(chip), :], preferred_element_type=F32)
        main, extra = term[:rows], term[rows:]
        for o in range(halves):
            main = main + pairs[step * halves + o][0] * extra[o : o + 1]
        lifted = main if lifted is None else lifted + main
        fixed = extra if fixed is None else fixed + extra
    average, scale = combine(pairs)
    slope = sum(fixed[o : o + 1] for o in range(halves))
    lifted = scale * (lifted - average * slope) + (fixed[halves : halves + 1] + fixed[halves + 1 : halves + 2])
    hidden = jnp.square(jnp.maximum(lifted, 0.0)).astype(BF16)
    normed = ((residual - average) * scale * gain1_v[...] + shift1_v[...]).astype(BF16)

    def block_of(chip, core):
        return pl.ds(pl.multiple_of((chip * halves + core) * cols, cols), cols)

    for copy in down_loads:
        copy.wait()
    for step in range(top, -1, -1):
        chip = chips[step]
        both = jnp.dot(hidden, down_v[:, chunk(chip)], preferred_element_type=F32)
        if step:
            for core in range(halves):
                o = (top - step) * halves + core
                p_send[o] = both[:, core * cols : (core + 1) * cols].astype(BF16)
                copy = remote(p_send.at[o], p_recv.at[me], p_ss.at[o], p_rs.at[me], chip, core)
                copy.start()
                pending.append(copy)
        else:
            both_v[...] = both
    for o, core in enumerate(cores[1:]):
        p_send[top * halves + o] = both_v[:, block_of(0, core)].astype(BF16)
        copy = remote(
            p_send.at[top * halves + o], p_recv.at[me], p_ss.at[top * halves + o], p_rs.at[me], my_kv, core
        )
        copy.start()
        pending.append(copy)
    total = both_v[:, block_of(0, my_tp)]
    total = total + ALPHA * normed.astype(F32)
    for chip, core in everyone():
        collect(p_recv, p_rs, chip, core)
        total = total + p_recv[chip * halves + core].astype(F32)
    center, moved, power = moments(total)
    finals_v[me] = as_row(center, power)
    spread(finals_v, f_ss, f_rs)
    pairs = [(center, power)]
    loads["g2"].wait()
    loads["s2"].wait()
    for chip, core in reversed(everyone()):
        collect(finals_v, f_rs, chip, core)
        pairs.append(as_columns(finals_v[chip * halves + core]))
    average, scale = combine(pairs)
    out[...] = ((total - average) * scale * gain2_v[...] + shift2_v[...]).astype(BF16)

    each_own(True, lambda copy: copy.wait_send())
    each_own(False, lambda copy: copy.wait_send())
    for copy in pending:
        copy.wait_send()


def finish_kernel(result, fresh, out, states_out, sems):
    puts = [
        pltpu.make_async_copy(fresh, states_out, sems.at[0]),
        pltpu.make_async_copy(result, out, sems.at[1]),
    ]
    for put in puts:
        put.start()
    for put in puts:
        put.wait()


def fused(groups, halves, *arrays):
    (tokens, wq, wk, wv, wg, wd, bias, states, head_gain, wout, gain1, shift1, wup, wdown, gain2,
     shift2) = arrays

    def flat(weight):
        return weight.transpose(1, 2, 0).reshape(-1, weight.shape[0])

    def row(vector):
        return vector.reshape(1, -1)

    rows, cols = tokens.shape
    members = groups * halves
    width = wq.shape[0]
    seqs, heads, kdim, vdim = states.shape
    proj = 3 * wq.shape[1] * wq.shape[2] + 2 * wv.shape[1] * wv.shape[2]
    vmem = pltpu.VMEM
    dma = pltpu.SemaphoreType.DMA
    anywhere = pl.BlockSpec(memory_space=pl.ANY)
    inside = pl.BlockSpec(memory_space=pltpu.VMEM)
    scratch = [
        vmem((proj, width), BF16),
        vmem(wout.shape, BF16),
        vmem(wup.shape, BF16),
        vmem(wdown.shape, BF16),
        vmem(states.shape, F32),
        vmem(bias.shape, F32),
        vmem(head_gain.shape, F32),
        vmem((1, cols), F32),
        vmem((1, cols), F32),
        vmem((1, cols), F32),
        vmem((1, cols), F32),
        vmem((rows, heads * kdim // groups), F32),
        vmem((members, rows, cols), BF16),
        vmem((rows, proj), F32),
        vmem((groups, seqs, proj), BF16),
        vmem((groups, seqs, proj), BF16),
        vmem((rows, proj), F32),
        vmem((seqs, heads * vdim), BF16),
        vmem((members, seqs, heads * vdim), BF16),
        vmem((rows, halves * heads * vdim), F32),
        vmem((groups, seqs, cols), F32),
        vmem((members, rows, cols), BF16),
        vmem((members, rows, cols), BF16),
        vmem((members, 1, 128), F32),
        vmem((rows, halves * cols), F32),
        vmem((members - 1, rows, cols), BF16),
        vmem((members, rows, cols), BF16),
        vmem((members, 1, 128), F32),
        dma((9,)),
        dma((groups, 5)),
        dma((groups,)),
        dma((4,)),
        pltpu.SemaphoreType.REGULAR((groups,)),
        dma((2 * groups * halves,)),
        dma((members,)),
        dma((groups,)),
        dma((groups,)),
    ]
    scratch += [dma((members,))] * 12
    result, fresh = pl.pallas_call(
        functools.partial(layer_kernel, groups, halves),
        out_shape=(
            vmem(tokens.shape, BF16),
            vmem(states.shape, F32),
        ),
        in_specs=[anywhere] * 16,
        out_specs=(inside, inside),
        scratch_shapes=scratch,
        compiler_params=pltpu.CompilerParams(
            collective_id=0, has_side_effects=True, vmem_limit_bytes=58*1024*1024
        ),
    )(
        tokens, flat(wq), flat(wk), flat(wd), flat(wv), flat(wg), bias, states, head_gain, wout,
        row(gain1), row(shift1), wup, wdown, row(gain2), row(shift2),
    )
    return pl.pallas_call(
        finish_kernel,
        out_shape=(
            jax.ShapeDtypeStruct(tokens.shape, BF16),
            jax.ShapeDtypeStruct(states.shape, F32),
        ),
        in_specs=[anywhere] * 2,
        out_specs=(anywhere, anywhere),
        scratch_shapes=[dma((2,))],
        compiler_params=pltpu.CompilerParams(vmem_limit_bytes=1048576),
    )(result, fresh)


def dispatch(groups, halves, *arrays):
    rows, cols = arrays[0].shape
    if rows == 8 and cols % 128 == 0 and rows % groups == 0 and groups > 2 and halves <= 4:
        return fused(groups, halves, *arrays)
    return body(*arrays)


def solution(mesh):
    placed = (
        P("dp", ("kv", "tp")),
        P(None, "tp", "kv"),
        P(None, "tp", "kv"),
        P(None, "tp", "kv"),
        P(None, "tp", "kv"),
        P(None, "tp", "kv"),
        P("tp", None),
        P(("dp", "kv"), "tp", None, None),
        P("tp", None),
        P(None, ("kv", "tp")),
        P(("kv", "tp")),
        P(("kv", "tp")),
        P(None, ("kv", "tp")),
        P(("kv", "tp"), None),
        P(("kv", "tp")),
        P(("kv", "tp")),
    )
    return jax.shard_map(
        functools.partial(dispatch, mesh.shape["kv"], mesh.shape["tp"]),
        mesh=mesh,
        in_specs=placed,
        out_specs=(P("dp", ("kv", "tp")), P(("dp", "kv"), "tp", None, None)),
        check_vma=False,
    )
```

time: 44.2 us -> 37.7 us (0.85)
  Pallas kernels: 43.4 us -> 36.9 us
    pallas_call x1, Pallas kernels: 40.9 us -> 35.6 us  [fused(): pl.pallas_call(functools.partial(layer_kernel, groups, halves), out_shape...]
    pallas_call x1, Pallas kernels: 2.43 us -> 1.34 us  [fused(): pl.pallas_call(finish_kernel, out_shape=(jax.ShapeDtypeStruct(tokens.shap...]
where the time goes in v1:
time: 37.7 us; the launch traced here: 37.6 us
  Pallas kernels  36.9 us (98%)
  between operations  0.64 us (2%)
    pallas_call x1, Pallas kernels, fused(): pl.pallas_call(functools.partial(layer_kernel, groups, halves), out_shape...  35.6 us
    pallas_call x1, Pallas kernels, fused(): pl.pallas_call(finish_kernel, out_shape=(jax.ShapeDtypeStruct(tokens.shap...  1.34 us

profile of v1, /device:TPU:0, one launch (start us, length us, event | category | flops | bytes accessed | tf_op | source)
XLA Modules:
  0.0 37.6 jit_solution(7149209270384941418)
XLA Ops:
  0.6 35.6 %shard_map.167 = (bf16[8,512]{1,0:T(8,128)(2,1)S(1)}, f32[2,8,128,256]{3,2,1,0:T(8,128)S(1)}) custom-call(bf16[8,512]{1,0:T(8,128)(2,1)} %tokens.1, bf16[256,4096]{1,0:T(8,128)(2,1)} %bitcast.21, bf16[256,4096]{1,0:T(8,128)(2,1)} %bitcast.22, bf16[256,4096]{1,0:T(8,128)(2,1)} %bitcast.23, bf16[512,4096]{1,0:T(8,128)(2,1)} %bitcast.19, ...), custom_call_target="tpu_custom_call" | custom-call | tf_op jit(solution)/shard_map/pallas_call | solution.py:577
  36.3 1.3 %shard_map.168 = (bf16[8,512]{1,0:T(8,128)(2,1)}, f32[2,8,128,256]{3,2,1,0:T(8,128)}) custom-call(bf16[8,512]{1,0:T(8,128)(2,1)S(1)} %get-tuple-element.4.result, f32[2,8,128,256]{3,2,1,0:T(8,128)S(1)} %get-tuple-element.5.fresh), custom_call_target="tpu_custom_call" | custom-call | tf_op jit(solution)/shard_map/pallas_call | solution.py:593

commit v2 on v1

--- a/solution.py
+++ b/solution.py
@@ -122,11 +122,11 @@
     return lax.dot_general(left, right, (((1,), (1,)), ((), ())), preferred_element_type=F32)
 
 
-def nearest(place, count, step):
+def nearest(place, count, step, lower):
     below, above = place, count - 1 - place
     pairs = jnp.minimum(below, above)
     away = (step + 1) // 2 * (1 if step % 2 else -1)
-    zigzag = jnp.where(below <= above, place - away, place + away)
+    zigzag = jnp.where(lower, place - away, place + away)
     onward = jnp.where(below < above, place + (step - pairs), place - (step - pairs))
     return jnp.where(step <= 2 * pairs, zigzag, onward)
 
@@ -152,7 +152,10 @@
     kc, vc = kdim // groups, vdim // groups
     nk, nv = heads * kc, heads * vc
     top = groups - 1
-    chips = [nearest(my_kv, groups, step) for step in range(groups)]
+    low_half = 2 * my_kv <= top
+    rising = [nearest(my_kv, groups, step, my_kv >= 0) for step in range(groups)]
+    chips = [nearest(my_kv, groups, step, low_half) for step in range(groups)]
+    inward = [nearest(my_kv, groups, step, jnp.logical_not(low_half)) for step in range(groups)]
     cores = [lax.rem(my_tp + o, halves) for o in range(halves)]
 
     def load(src, dst, sem):
@@ -180,7 +183,7 @@
             ))
             start += size
 
-    load_projections(0, chips[0])
+    load_projections(0, rising[0])
     barrier = pltpu.get_barrier_semaphore()
 
     def greet(kv, tp):
@@ -193,7 +196,7 @@
 
     for core in cores[1:]:
         greet(my_kv, core)
-    for d in range(1, groups):
+    for d in range(2, groups):
 
         @pl.when(my_kv + d < groups)
         def _():
@@ -214,12 +217,14 @@
         if first:
             for o, core in enumerate(cores):
                 plans.append((my_kv < top, my_kv + 1, core, o))
-            for d in range(top, 0, -1):
+            for d in range(top, 1, -1):
                 for o, core in enumerate(cores):
                     plans.append((my_kv >= d, my_kv - d, core, (d + 1) * halves + o))
             for o, core in enumerate(cores[1:]):
                 plans.append((None, my_kv, core, halves + o))
         else:
+            for o, core in enumerate(cores):
+                plans.append((my_kv > 0, my_kv - 1, core, 2 * halves + o))
             for d in range(2, groups):
                 for o, core in enumerate(cores):
                     plans.append((my_kv + d < groups, my_kv + d, core, (groups + d - 1) * halves + o))
@@ -235,8 +240,13 @@
                 def _():
                     act(own_copy(kv, core, slot))
 
+    def send_below():
+        pl.semaphore_wait(ready.at[1], halves)
+        for o, core in enumerate(cores):
+            own_copy(my_kv - 1, core, 2 * halves + o).start()
+
     def send_far():
-        for d in range(2, groups):
+        for d in range(top, 1, -1):
 
             @pl.when(my_kv + d < groups)
             def _():
@@ -244,7 +254,7 @@
                 for o, core in enumerate(cores):
                     own_copy(my_kv + d, core, (groups + d - 1) * halves + o).start()
 
-    expected = (halves - 1) + halves * my_kv + jnp.where(my_kv < top, halves, 0)
+    expected = (halves - 1) + halves * jnp.maximum(my_kv - 1, 0) + jnp.where(my_kv < top, halves, 0)
     pl.semaphore_wait(barrier, expected)
     for d in range(2, groups):
 
@@ -255,13 +265,20 @@
                     ready.at[d], inc=1, device_id={"kv": my_kv - d, "tp": core}, device_id_type=MESH
                 )
 
+    @pl.when(my_kv < top)
+    def _():
+        for core in cores:
+            pl.semaphore_signal(
+                ready.at[1], inc=1, device_id={"kv": my_kv + 1, "tp": core}, device_id_type=MESH
+            )
+
     loads["tok"].wait()
     each_own(True, lambda copy: copy.start())
-    load_projections(1, chips[1])
+    load_projections(1, rising[1])
     pending = []
 
     def everyone():
-        targets = [(chip, core) for chip in reversed(chips[1:]) for core in cores]
+        targets = [(chip, core) for chip in reversed(chips[1:]) for core in range(halves)]
         return targets + [(my_kv, core) for core in cores[1:]]
 
     def spread(buffer, send, recv):
@@ -275,13 +292,13 @@
         remote(buffer.at[block], buffer.at[block], recv.at[block], recv.at[block], my_kv, my_tp).wait_recv()
 
     late = []
-    for step, chip in enumerate(chips):
+    for step, chip in enumerate(rising):
         for core in cores if step else cores[1:]:
             collect(x_v, x_rs, chip, core)
         for index in range(5):
             proj_loads[step * 5 + index].wait()
         if step + 2 < groups:
-            load_projections(step + 2, chips[step + 2])
+            load_projections(step + 2, rising[step + 2])
         if step == max(groups - 2, 0):
             for index, (name, src, dst) in enumerate((
                 ("hg", head_gain, hgain_v), ("g2", gain2, gain2_v), ("s2", shift2, shift2_v),
@@ -289,14 +306,29 @@
             )):
                 loads[name] = load(src, dst, load_sem.at[4 + index])
         if step == groups - 1:
-            for index, to in enumerate(chips):
+            for index, to in enumerate(inward):
                 late.append(load(wup.at[chunk(to), :], up_v.at[chunk(to), :], up_sem.at[index]))
-        blocks = x_v[pl.ds(chip * halves, halves)]
-        left = jnp.concatenate([blocks[o] for o in range(halves)], axis=1)
-        term = dot_nt(left, proj_v[:, chunk(chip)])
-        acc_v[...] = acc_v[...] + term if step else term
+
         if step == 0:
-            send_far()
+
+            @pl.when(my_kv > 0)
+            def _():
+                send_below()
+                send_far()
+
+        @pl.when(my_kv >= 0)
+        def _():
+            blocks = x_v[pl.ds(chip * halves, halves)]
+            left = jnp.concatenate([blocks[o] for o in range(halves)], axis=1)
+            term = dot_nt(left, proj_v[:, chunk(chip)])
+            acc_v[...] = acc_v[...] + term if step else term
+
+        if step == 0:
+
+            @pl.when(my_kv == 0)
+            def _():
+                send_far()
+
             loads["g1"].wait()
             loads["s1"].wait()
             loads["bias"].wait()
@@ -356,14 +388,17 @@
         value = jnp.concatenate([wide(s, h, 3 * nk) for h in range(heads)], axis=0)
         gate = jnp.concatenate([wide(s, h, 3 * nk + nv) for h in range(heads)], axis=0)
         values.append(value)
-        lines = []
-        for h in range(heads):
-            total = None
-            for b in range(groups):
-                lane = b * seqs + s
-                term = turned[h * kc : (h + 1) * kc, lane : lane + 1] * state_v[s, h, b * kc : (b + 1) * kc, :]
-                total = term if total is None else total + term
-            lines.append(jnp.sum(total, axis=0, keepdims=True))
+        totals = [None] * heads
+        for b in range(groups):
+            lane = b * seqs + s
+            column = jnp.broadcast_to(turned[0:nk, lane : lane + 1], (nk, 128))
+            for h in range(heads):
+                for low in range(0, kc, 8):
+                    block = state_v[s, h, b * kc + low : b * kc + low + 8, :]
+                    part = column[h * kc + low : h * kc + low + 8]
+                    term = jnp.concatenate([part] * (vdim // 128), axis=1) * block
+                    totals[h] = term if totals[h] is None else totals[h] + term
+        lines = [jnp.sum(total, axis=0, keepdims=True) for total in totals]
         readout = jnp.concatenate(lines, axis=0) + strength[:, s : s + 1] * value
         power = jnp.mean(readout * readout, axis=-1, keepdims=True)
         readout = readout * lax.rsqrt(power + RMS_EPS) * hgain_v[...]
@@ -395,10 +430,14 @@
         for core in cores if step else cores[1:]:
             collect(att_recv, t_rs, chip, core)
         for t in range(halves):
-            x_rows[step * seqs : (step + 1) * seqs, t * half : (t + 1) * half] = att_recv[chip * halves + t].astype(F32)
-    mixed = jnp.dot(x_rows[...].astype(BF16), out_v[...], preferred_element_type=F32)
-    for step, chip in enumerate(chips):
-        mixed_v[chip] = mixed[step * seqs : (step + 1) * seqs]
+            x_rows[step * seqs : (step + 1) * seqs, t * half : (t + 1) * half] = att_recv[chip * halves + t]
+
+    @pl.when(my_kv >= 0)
+    def _():
+        mixed = jnp.dot(x_rows[...], out_v[...], preferred_element_type=F32)
+        for step, chip in enumerate(chips):
+            mixed_v[chip] = mixed[step * seqs : (step + 1) * seqs]
+
     mixed = jnp.concatenate([mixed_v[a] for a in range(groups)], axis=0)
     residual = ALPHA * x_v[me].astype(F32) + mixed
 
@@ -427,15 +466,15 @@
     center, moved, power = moments(residual)
     u_v[me] = (moved * gain1_v[...]).astype(BF16)
     moments_v[me] = as_row(center, power)
+    spread(moments_v, m_ss, m_rs)
     spread(u_v, u_ss, u_rs)
-    spread(moments_v, m_ss, m_rs)
 
     for step, chip in enumerate(chips):
         for core in cores if step else cores[1:]:
             collect(const_v, c_rs, chip, core)
     lifted = fixed = None
     pairs = []
-    for step, chip in enumerate(chips):
+    for step, chip in enumerate(inward):
         late[step].wait()
         for core in cores if step else cores[1:]:
             collect(u_v, u_rs, chip, core)
@@ -462,25 +501,19 @@
 
     for copy in down_loads:
         copy.wait()
-    for step in range(top, -1, -1):
-        chip = chips[step]
-        both = jnp.dot(hidden, down_v[:, chunk(chip)], preferred_element_type=F32)
-        if step:
-            for core in range(halves):
-                o = (top - step) * halves + core
-                p_send[o] = both[:, core * cols : (core + 1) * cols].astype(BF16)
-                copy = remote(p_send.at[o], p_recv.at[me], p_ss.at[o], p_rs.at[me], chip, core)
-                copy.start()
-                pending.append(copy)
-        else:
-            both_v[...] = both
-    for o, core in enumerate(cores[1:]):
-        p_send[top * halves + o] = both_v[:, block_of(0, core)].astype(BF16)
-        copy = remote(
-            p_send.at[top * halves + o], p_recv.at[me], p_ss.at[top * halves + o], p_rs.at[me], my_kv, core
-        )
+    def send_sum(o, value, chip, core):
+        p_send[o] = value.astype(BF16)
+        copy = remote(p_send.at[o], p_recv.at[me], p_ss.at[o], p_rs.at[me], chip, core)
         copy.start()
         pending.append(copy)
+
+    for step in range(top, 0, -1):
+        both = jnp.dot(hidden, down_v[:, chunk(chips[step])], preferred_element_type=F32)
+        for core in range(halves):
+            send_sum((top - step) * halves + core, both[:, core * cols : (core + 1) * cols], chips[step], core)
+    both_v[...] = jnp.dot(hidden, down_v[:, chunk(my_kv)], preferred_element_type=F32)
+    for o, core in enumerate(cores[1:]):
+        send_sum(top * halves + o, both_v[:, block_of(0, core)], my_kv, core)
     total = both_v[:, block_of(0, my_tp)]
     total = total + ALPHA * normed.astype(F32)
     for chip, core in everyone():
@@ -554,7 +587,7 @@
         vmem((rows, proj), F32),
         vmem((seqs, heads * vdim), BF16),
         vmem((members, seqs, heads * vdim), BF16),
-        vmem((rows, halves * heads * vdim), F32),
+        vmem((rows, halves * heads * vdim), BF16),
         vmem((groups, seqs, cols), F32),
         vmem((members, rows, cols), BF16),
         vmem((members, rows, cols), BF16),

time: 37.7 us -> 36.2 us (0.960)
  Pallas kernels: 36.9 us -> 35.4 us
    pallas_call x1, Pallas kernels: 35.6 us -> 34.1 us  [fused(): pl.pallas_call(functools.partial(layer_kernel, groups, halves), out_shape...]
where the time goes in v2:
time: 36.2 us; the launch traced here: 36.1 us
  Pallas kernels  35.4 us (98%)
  between operations  0.64 us (2%)
    pallas_call x1, Pallas kernels, fused(): pl.pallas_call(functools.partial(layer_kernel, groups, halves), out_shape...  34.1 us
    pallas_call x1, Pallas kernels, fused(): pl.pallas_call(finish_kernel, out_shape=(jax.ShapeDtypeStruct(tokens.shap...  1.34 us

profile of v2, /device:TPU:0, one launch (start us, length us, event | category | flops | bytes accessed | tf_op | source)
XLA Modules:
  0.0 36.1 jit_solution(6646567940625436470)
XLA Ops:
  0.6 34.1 %shard_map.167 = (bf16[8,512]{1,0:T(8,128)(2,1)S(1)}, f32[2,8,128,256]{3,2,1,0:T(8,128)S(1)}) custom-call(bf16[8,512]{1,0:T(8,128)(2,1)} %tokens.1, bf16[256,4096]{1,0:T(8,128)(2,1)} %bitcast.21, bf16[256,4096]{1,0:T(8,128)(2,1)} %bitcast.22, bf16[256,4096]{1,0:T(8,128)(2,1)} %bitcast.23, bf16[512,4096]{1,0:T(8,128)(2,1)} %bitcast.19, ...), custom_call_target="tpu_custom_call" | custom-call | tf_op jit(solution)/shard_map/pallas_call | solution.py:610
  34.7 1.3 %shard_map.168 = (bf16[8,512]{1,0:T(8,128)(2,1)}, f32[2,8,128,256]{3,2,1,0:T(8,128)}) custom-call(bf16[8,512]{1,0:T(8,128)(2,1)S(1)} %get-tuple-element.4.result, f32[2,8,128,256]{3,2,1,0:T(8,128)S(1)} %get-tuple-element.5.fresh), custom_call_target="tpu_custom_call" | custom-call | tf_op jit(solution)/shard_map/pallas_call | solution.py:626

commit v3 on v2

--- a/solution.py
+++ b/solution.py
@@ -275,14 +275,23 @@
     loads["tok"].wait()
     each_own(True, lambda copy: copy.start())
     load_projections(1, rising[1])
+
+    @pl.when(my_kv > 0)
+    def _():
+        send_below()
+
     pending = []
 
     def everyone():
         targets = [(chip, core) for chip in reversed(chips[1:]) for core in range(halves)]
         return targets + [(my_kv, core) for core in cores[1:]]
 
-    def spread(buffer, send, recv):
-        for o, (chip, core) in enumerate(everyone()):
+    def near_first():
+        targets = [(chip, core) for chip in inward[1:] for core in range(halves)]
+        return [(my_kv, core) for core in cores[1:]] + targets
+
+    def spread(buffer, send, recv, targets=None):
+        for o, (chip, core) in enumerate(targets or everyone()):
             copy = remote(buffer.at[me], buffer.at[me], send.at[o], recv.at[me], chip, core)
             copy.start()
             pending.append(copy)
@@ -313,7 +322,6 @@
 
             @pl.when(my_kv > 0)
             def _():
-                send_below()
                 send_far()
 
         @pl.when(my_kv >= 0)
@@ -342,7 +350,7 @@
             for h in range(heads):
                 for b in range(groups):
                     piece = jnp.broadcast_to(bias_v[h : h + 1, b * kc : (b + 1) * kc], (seqs, kc))
-                    bias_rows[b * seqs : (b + 1) * seqs, h * kc : (h + 1) * kc] = piece
+                    bias_rows[b, :, h * kc : (h + 1) * kc] = piece
         if step == groups - 2:
             spread(const_v, c_ss, c_rs)
     quarter = down_v.shape[0] // 4
@@ -360,45 +368,46 @@
     a_recv[my_kv] = a_send[my_kv]
     loads["st"].wait()
     loads["hg"].wait()
-    for peer in chips[1:]:
-        remote(a_send.at[peer], a_recv.at[peer], a_ss.at[0], a_rs.at[peer], my_kv, my_tp).wait_recv()
+    def decay(z):
+        return jnp.exp((jnp.minimum(z, 0.0) - jnp.log1p(jnp.exp(-jnp.abs(z)))) / TAU)
+
+    totals = [[None] * heads for _ in range(seqs)]
+    strength = None
+    for step, peer in enumerate(chips):
+        if step:
+            remote(a_send.at[peer], a_recv.at[peer], a_ss.at[0], a_rs.at[peer], my_kv, my_tp).wait_recv()
+        got = a_recv[peer].astype(F32)
+        q = got[:, 0:nk] * KEY_DIM ** (-0.5)
+        turned = jnp.concatenate(
+            [q * decay(got[:, 2 * nk : 3 * nk] + bias_rows[peer]), q * got[:, nk : 2 * nk]], axis=1
+        ).T
+        met = jnp.concatenate(
+            [jnp.sum(turned[nk + h * kc : nk + (h + 1) * kc, :], axis=0, keepdims=True) for h in range(heads)],
+            axis=0,
+        )
+        strength = met if strength is None else strength + met
+        for s in range(seqs):
+            column = jnp.broadcast_to(turned[0:nk, s : s + 1], (nk, 128))
+            for h in range(heads):
+                for low in range(0, kc, 8):
+                    block = state_v[s, h, pl.ds(pl.multiple_of(peer * kc + low, 8), 8), :]
+                    part = column[h * kc + low : h * kc + low + 8]
+                    term = jnp.concatenate([part] * (vdim // 128), axis=1) * block
+                    totals[s][h] = term if totals[s][h] is None else totals[s][h] + term
     for b in range(groups):
         a_rows[b * seqs : (b + 1) * seqs, :] = a_recv[b].astype(F32)
-
-    q = a_rows[:, 0:nk] * KEY_DIM ** (-0.5)
-    k = a_rows[:, nk : 2 * nk]
-    z = a_rows[:, 2 * nk : 3 * nk] + bias_rows[...]
-    retain = jnp.exp((jnp.minimum(z, 0.0) - jnp.log1p(jnp.exp(-jnp.abs(z)))) / TAU)
-    product = q * k
-    met = product
-    for b in range(1, groups):
-        met = met + pltpu.roll(product, b * seqs, 0)
-    turned = jnp.concatenate([q * retain, met], axis=1).T
 
     def wide(s, h, first):
         start = first + h * vc
         parts = [a_rows[b * seqs + s : b * seqs + s + 1, start : start + vc] for b in range(groups)]
         return jnp.concatenate(parts, axis=1)
 
-    strength = jnp.concatenate(
-        [jnp.sum(turned[nk + h * kc : nk + (h + 1) * kc, :], axis=0, keepdims=True) for h in range(heads)], axis=0
-    )
     values = []
     for s in range(seqs):
         value = jnp.concatenate([wide(s, h, 3 * nk) for h in range(heads)], axis=0)
         gate = jnp.concatenate([wide(s, h, 3 * nk + nv) for h in range(heads)], axis=0)
         values.append(value)
-        totals = [None] * heads
-        for b in range(groups):
-            lane = b * seqs + s
-            column = jnp.broadcast_to(turned[0:nk, lane : lane + 1], (nk, 128))
-            for h in range(heads):
-                for low in range(0, kc, 8):
-                    block = state_v[s, h, b * kc + low : b * kc + low + 8, :]
-                    part = column[h * kc + low : h * kc + low + 8]
-                    term = jnp.concatenate([part] * (vdim // 128), axis=1) * block
-                    totals[h] = term if totals[h] is None else totals[h] + term
-        lines = [jnp.sum(total, axis=0, keepdims=True) for total in totals]
+        lines = [jnp.sum(total, axis=0, keepdims=True) for total in totals[s]]
         readout = jnp.concatenate(lines, axis=0) + strength[:, s : s + 1] * value
         power = jnp.mean(readout * readout, axis=-1, keepdims=True)
         readout = readout * lax.rsqrt(power + RMS_EPS) * hgain_v[...]
@@ -411,7 +420,9 @@
         pending.append(copy)
     att_recv[me] = att_send[...]
 
-    later = jnp.concatenate([retain, k], axis=1).T
+    slopes = jnp.concatenate([bias_rows[b] for b in range(groups)], axis=0)
+    retain = decay(a_rows[:, 2 * nk : 3 * nk] + slopes)
+    later = jnp.concatenate([retain, a_rows[:, nk : 2 * nk]], axis=1).T
     for s in range(seqs):
         for h in range(heads):
             for b in range(groups):
@@ -467,7 +478,7 @@
     u_v[me] = (moved * gain1_v[...]).astype(BF16)
     moments_v[me] = as_row(center, power)
     spread(moments_v, m_ss, m_rs)
-    spread(u_v, u_ss, u_rs)
+    spread(u_v, u_ss, u_rs, near_first())
 
     for step, chip in enumerate(chips):
         for core in cores if step else cores[1:]:
@@ -579,7 +590,7 @@
         vmem((1, cols), F32),
         vmem((1, cols), F32),
         vmem((1, cols), F32),
-        vmem((rows, heads * kdim // groups), F32),
+        vmem((groups, seqs, heads * kdim // groups), F32),
         vmem((members, rows, cols), BF16),
         vmem((rows, proj), F32),
         vmem((groups, seqs, proj), BF16),

time: 36.2 us -> 35.1 us (0.970)
  Pallas kernels: 35.4 us -> 34.3 us
    pallas_call x1, Pallas kernels: 34.1 us -> 32.9 us  [fused(): pl.pallas_call(functools.partial(layer_kernel, groups, halves), out_shape...]
where the time goes in v3:
time: 35.1 us; the launch traced here: 34.9 us
  Pallas kernels  34.3 us (98%)
  between operations  0.64 us (2%)
    pallas_call x1, Pallas kernels, fused(): pl.pallas_call(functools.partial(layer_kernel, groups, halves), out_shape...  32.9 us
    pallas_call x1, Pallas kernels, fused(): pl.pallas_call(finish_kernel, out_shape=(jax.ShapeDtypeStruct(tokens.shap...  1.34 us

profile of v3, /device:TPU:0, one launch (start us, length us, event | category | flops | bytes accessed | tf_op | source)
XLA Modules:
  0.0 34.9 jit_solution(11317487686750670579)
XLA Ops:
  0.6 32.9 %shard_map.167 = (bf16[8,512]{1,0:T(8,128)(2,1)S(1)}, f32[2,8,128,256]{3,2,1,0:T(8,128)S(1)}) custom-call(bf16[8,512]{1,0:T(8,128)(2,1)} %tokens.1, bf16[256,4096]{1,0:T(8,128)(2,1)} %bitcast.21, bf16[256,4096]{1,0:T(8,128)(2,1)} %bitcast.22, bf16[256,4096]{1,0:T(8,128)(2,1)} %bitcast.23, bf16[512,4096]{1,0:T(8,128)(2,1)} %bitcast.19, ...), custom_call_target="tpu_custom_call" | custom-call | tf_op jit(solution)/shard_map/pallas_call | solution.py:621
  33.6 1.3 %shard_map.168 = (bf16[8,512]{1,0:T(8,128)(2,1)}, f32[2,8,128,256]{3,2,1,0:T(8,128)}) custom-call(bf16[8,512]{1,0:T(8,128)(2,1)S(1)} %get-tuple-element.4.result, f32[2,8,128,256]{3,2,1,0:T(8,128)S(1)} %get-tuple-element.5.fresh), custom_call_target="tpu_custom_call" | custom-call | tf_op jit(solution)/shard_map/pallas_call | solution.py:637

commit v4 on v3

--- a/solution.py
+++ b/solution.py
@@ -373,7 +373,7 @@
 
     totals = [[None] * heads for _ in range(seqs)]
     strength = None
-    for step, peer in enumerate(chips):
+    for step, peer in enumerate(inward):
         if step:
             remote(a_send.at[peer], a_recv.at[peer], a_ss.at[0], a_rs.at[peer], my_kv, my_tp).wait_recv()
         got = a_recv[peer].astype(F32)
@@ -455,11 +455,6 @@
     lane = lax.broadcasted_iota(jnp.int32, (rows, 128), 1)
     line = lax.broadcasted_iota(jnp.int32, (rows, 128), 0)
 
-    def moments(block):
-        center = jnp.sum(block, axis=-1, keepdims=True) / cols
-        moved = block - center
-        return center, moved, jnp.sum(moved * moved, axis=-1, keepdims=True)
-
     def as_row(center, power):
         both = jnp.where(lane == line, center, 0.0) + jnp.where(lane == line + rows, power, 0.0)
         return jnp.sum(both, axis=0, keepdims=True)
@@ -474,8 +469,9 @@
         powers = sum(power + cols * jnp.square(center - average) for center, power in pairs)
         return average, lax.rsqrt(powers / width + LN_EPS)
 
-    center, moved, power = moments(residual)
-    u_v[me] = (moved * gain1_v[...]).astype(BF16)
+    center = jnp.sum(residual, axis=-1, keepdims=True) / cols
+    power = jnp.sum(residual * residual, axis=-1, keepdims=True) - cols * center * center
+    u_v[me] = ((residual - center) * gain1_v[...]).astype(BF16)
     moments_v[me] = as_row(center, power)
     spread(moments_v, m_ss, m_rs)
     spread(u_v, u_ss, u_rs, near_first())
@@ -519,9 +515,9 @@
         pending.append(copy)
 
     for step in range(top, 0, -1):
-        both = jnp.dot(hidden, down_v[:, chunk(chips[step])], preferred_element_type=F32)
+        both = jnp.dot(hidden, down_v[:, chunk(inward[step])], preferred_element_type=F32)
         for core in range(halves):
-            send_sum((top - step) * halves + core, both[:, core * cols : (core + 1) * cols], chips[step], core)
+            send_sum((top - step) * halves + core, both[:, core * cols : (core + 1) * cols], inward[step], core)
     both_v[...] = jnp.dot(hidden, down_v[:, chunk(my_kv)], preferred_element_type=F32)
     for o, core in enumerate(cores[1:]):
         send_sum(top * halves + o, both_v[:, block_of(0, core)], my_kv, core)
@@ -530,16 +526,19 @@
     for chip, core in everyone():
         collect(p_recv, p_rs, chip, core)
         total = total + p_recv[chip * halves + core].astype(F32)
-    center, moved, power = moments(total)
-    finals_v[me] = as_row(center, power)
+    sums = jnp.sum(total, axis=-1, keepdims=True)
+    squares = jnp.sum(total * total, axis=-1, keepdims=True)
+    finals_v[me] = as_row(sums, squares)
     spread(finals_v, f_ss, f_rs)
-    pairs = [(center, power)]
     loads["g2"].wait()
     loads["s2"].wait()
+    gathered = finals_v[me]
     for chip, core in reversed(everyone()):
         collect(finals_v, f_rs, chip, core)
-        pairs.append(as_columns(finals_v[chip * halves + core]))
-    average, scale = combine(pairs)
+        gathered = gathered + finals_v[chip * halves + core]
+    sums, squares = as_columns(gathered)
+    average = sums / width
+    scale = lax.rsqrt(squares / width - average * average + LN_EPS)
     out[...] = ((total - average) * scale * gain2_v[...] + shift2_v[...]).astype(BF16)
 
     each_own(True, lambda copy: copy.wait_send())

time: 35.1 us -> 34.7 us (0.989)
  Pallas kernels: 34.3 us -> 33.9 us
where the time goes in v4:
time: 34.7 us; the launch traced here: 34.6 us
  Pallas kernels  33.9 us (98%)
  between operations  0.64 us (2%)
    pallas_call x1, Pallas kernels, fused(): pl.pallas_call(functools.partial(layer_kernel, groups, halves), out_shape...  32.6 us
    pallas_call x1, Pallas kernels, fused(): pl.pallas_call(finish_kernel, out_shape=(jax.ShapeDtypeStruct(tokens.shap...  1.34 us

profile of v4, /device:TPU:0, one launch (start us, length us, event | category | flops | bytes accessed | tf_op | source)
XLA Modules:
  0.0 34.6 jit_solution(7938887864647140709)
XLA Ops:
  0.6 32.6 %shard_map.167 = (bf16[8,512]{1,0:T(8,128)(2,1)S(1)}, f32[2,8,128,256]{3,2,1,0:T(8,128)S(1)}) custom-call(bf16[8,512]{1,0:T(8,128)(2,1)} %tokens.1, bf16[256,4096]{1,0:T(8,128)(2,1)} %bitcast.21, bf16[256,4096]{1,0:T(8,128)(2,1)} %bitcast.22, bf16[256,4096]{1,0:T(8,128)(2,1)} %bitcast.23, bf16[512,4096]{1,0:T(8,128)(2,1)} %bitcast.19, ...), custom_call_target="tpu_custom_call" | custom-call | tf_op jit(solution)/shard_map/pallas_call | solution.py:620
  33.2 1.3 %shard_map.168 = (bf16[8,512]{1,0:T(8,128)(2,1)}, f32[2,8,128,256]{3,2,1,0:T(8,128)}) custom-call(bf16[8,512]{1,0:T(8,128)(2,1)S(1)} %get-tuple-element.4.result, f32[2,8,128,256]{3,2,1,0:T(8,128)S(1)} %get-tuple-element.5.fresh), custom_call_target="tpu_custom_call" | custom-call | tf_op jit(solution)/shard_map/pallas_call | solution.py:636

commit v5 on v4

--- a/solution.py
+++ b/solution.py
@@ -351,7 +351,7 @@
                 for b in range(groups):
                     piece = jnp.broadcast_to(bias_v[h : h + 1, b * kc : (b + 1) * kc], (seqs, kc))
                     bias_rows[b, :, h * kc : (h + 1) * kc] = piece
-        if step == groups - 2:
+        if step == groups - 3:
             spread(const_v, c_ss, c_rs)
     quarter = down_v.shape[0] // 4
     down_loads = [
@@ -518,10 +518,10 @@
         both = jnp.dot(hidden, down_v[:, chunk(inward[step])], preferred_element_type=F32)
         for core in range(halves):
             send_sum((top - step) * halves + core, both[:, core * cols : (core + 1) * cols], inward[step], core)
-    both_v[...] = jnp.dot(hidden, down_v[:, chunk(my_kv)], preferred_element_type=F32)
     for o, core in enumerate(cores[1:]):
-        send_sum(top * halves + o, both_v[:, block_of(0, core)], my_kv, core)
-    total = both_v[:, block_of(0, my_tp)]
+        part = jnp.dot(hidden, down_v[:, block_of(my_kv, core)], preferred_element_type=F32)
+        send_sum(top * halves + o, part, my_kv, core)
+    total = jnp.dot(hidden, down_v[:, block_of(my_kv, my_tp)], preferred_element_type=F32)
     total = total + ALPHA * normed.astype(F32)
     for chip, core in everyone():
         collect(p_recv, p_rs, chip, core)

time: 34.7 us -> 34.7 us (level)
  no operation moved by 1% of the time
where the time goes in v5:
time: 34.7 us; the launch traced here: 34.6 us
  Pallas kernels  33.9 us (98%)
  between operations  0.64 us (2%)
    pallas_call x1, Pallas kernels, fused(): pl.pallas_call(functools.partial(layer_kernel, groups, halves), out_shape...  32.6 us
    pallas_call x1, Pallas kernels, fused(): pl.pallas_call(finish_kernel, out_shape=(jax.ShapeDtypeStruct(tokens.shap...  1.34 us

profile of v5, /device:TPU:0, one launch (start us, length us, event | category | flops | bytes accessed | tf_op | source)
XLA Modules:
  0.0 34.6 jit_solution(11575229678391944657)
XLA Ops:
  0.6 32.6 %shard_map.167 = (bf16[8,512]{1,0:T(8,128)(2,1)S(1)}, f32[2,8,128,256]{3,2,1,0:T(8,128)S(1)}) custom-call(bf16[8,512]{1,0:T(8,128)(2,1)} %tokens.1, bf16[256,4096]{1,0:T(8,128)(2,1)} %bitcast.21, bf16[256,4096]{1,0:T(8,128)(2,1)} %bitcast.22, bf16[256,4096]{1,0:T(8,128)(2,1)} %bitcast.23, bf16[512,4096]{1,0:T(8,128)(2,1)} %bitcast.19, ...), custom_call_target="tpu_custom_call" | custom-call | tf_op jit(solution)/shard_map/pallas_call | solution.py:620
  33.2 1.3 %shard_map.168 = (bf16[8,512]{1,0:T(8,128)(2,1)}, f32[2,8,128,256]{3,2,1,0:T(8,128)}) custom-call(bf16[8,512]{1,0:T(8,128)(2,1)S(1)} %get-tuple-element.4.result, f32[2,8,128,256]{3,2,1,0:T(8,128)S(1)} %get-tuple-element.5.fresh), custom_call_target="tpu_custom_call" | custom-call | tf_op jit(solution)/shard_map/pallas_call | solution.py:636
